TPU v7x, 32 devices: a whole 2x2x4 slice. The times are simulated.
32 devices in a mesh: sp: 8 (over z, x), tp: 4 (over y, core).
Axes of the slice: x: 2, y: 2, z: 4, core: 2. Of those that a mesh axis runs over, the one named last changes fastest.
Arguments:
- tokens: bfloat16 [4096, 2048], P(('sp', 'tp')), may hold values from -6 to 6
- norm_gain: float32 [2048], replicated, may hold values from 0.1 to 1.9
- pool_in_weight: bfloat16 [2048, 1024], P('sp', 'tp'), may hold values from -0.125 to 0.125
- query_weight: bfloat16 [2048, 1024], P('sp', 'tp'), may hold values from -0.125 to 0.125
- forget_weight: bfloat16 [2048, 1024], P('sp', 'tp'), may hold values from -0.125 to 0.125
- input_weight: bfloat16 [2048, 1024], P('sp', 'tp'), may hold values from -0.125 to 0.125
- forget_gap: float32 [1024], P('tp'), may hold values from 0 to 0.02
- decay_shift: float32 [8, 4096], P('tp', 'sp'), may hold values from -0.42 to 0
- out_gain: float32 [128], replicated, may hold values from 0.1 to 1.9
- pool_out_weight: bfloat16 [1024, 2048], P('tp', 'sp'), may hold values from -0.53033009 to 0.53033009
- recur_out_weight: bfloat16 [1024, 2048], P('tp', 'sp'), may hold values from -0.53033009 to 0.53033009
Outputs:
- mixed_out: bfloat16 [4096, 2048], P(('sp', 'tp'))
All inputs are finite; a program needn't handle non-finite values.
Results may differ from a plain program's by a relative error of at most 0.014.
Values may be sent and summed in bfloat16 or wider, within the bound.
A program may use at most 64 MiB of HBM per device.

v0:
```python
import jax
import jax.numpy as jnp
from jax import lax
from jax.sharding import PartitionSpec as P

GROUPS = 4
RDIM = 128
SPAN = 64
EPSILON = 1e-06
EXACT_MATMUL = lax.Precision.HIGHEST


def passed_along(block, axis, distance):
    devices = range(lax.axis_size(axis))
    route = [(i - distance, i) for i in devices if i - distance in devices]
    return lax.ppermute(block, axis, route)


def prefix(part, axis, combine, identity):
    place = lax.axis_index(axis)
    gathered = jax.tree.map(lambda a: lax.all_gather(a, axis), part)
    state = jax.tree.map(lambda a, e: jnp.zeros_like(a) + jnp.asarray(e, a.dtype), part, identity)

    def one(hop, state):
        return combine(
            state, jax.tree.map(lambda a: lax.dynamic_index_in_dim(a, hop, 0, False), gathered)
        )

    return lax.fori_loop(0, place, one, state)


def window_sums(padded, levels, reach):
    length = padded.shape[0] - reach
    results = []
    running = padded
    for level in range(levels):
        width = 2**level
        running = running[width:] + running[:-width]
        offset = reach + 1 - 2 * width
        results.append(lax.slice_in_dim(running, offset, offset + length, axis=0))
    return results


def chain(earlier, later):
    return (earlier[0] * later[0], later[0][:, :, None] * earlier[1] + later[1])


def to_blocks(tensor, block_count, head_count):
    return tensor.reshape(block_count, SPAN, head_count, RDIM).transpose(0, 2, 1, 3)


def local(
    tokens,
    norm_gain,
    pool_in_weight,
    query_weight,
    forget_weight,
    input_weight,
    forget_gap,
    decay_shift,
    out_gain,
    pool_out_weight,
    recur_out_weight,
):
    pool_cols = pool_in_weight.shape[1]
    recur_cols = query_weight.shape[1]
    local_in = jnp.concatenate([pool_in_weight, query_weight, forget_weight, input_weight], axis=1)
    whole_in = lax.all_gather(local_in, "sp", axis=0, tiled=True)
    floats = tokens.astype(jnp.float32)
    scale = lax.rsqrt(jnp.mean(floats * floats, axis=-1, keepdims=True) + EPSILON)
    normed = (floats * scale * norm_gain).astype(jnp.bfloat16)
    pool_weight = whole_in[:, :pool_cols]
    recur_weight = whole_in[:, pool_cols:]
    pooled_in = jnp.dot(
        lax.all_gather(normed, "tp", axis=0, tiled=True),
        pool_weight,
        preferred_element_type=jnp.float32,
    ).astype(jnp.bfloat16)
    recur_in = jnp.dot(
        lax.all_gather(normed, "tp", axis=0, tiled=True),
        recur_weight,
        preferred_element_type=jnp.float32,
    ).astype(jnp.bfloat16)
    query = recur_in[:, :recur_cols].astype(jnp.float32)
    forget_pre = recur_in[:, recur_cols : 2 * recur_cols].astype(jnp.float32)
    values = recur_in[:, 2 * recur_cols :].astype(jnp.float32)
    row_count = pooled_in.shape[0]
    head_count = recur_cols // RDIM
    block_count = row_count // SPAN
    gate_pre = forget_pre.reshape(row_count, head_count, RDIM)
    opened = forget_gap.reshape(head_count, RDIM) * jax.nn.sigmoid(-gate_pre)
    log_decay = jnp.log1p(-opened) + decay_shift.T[:, :, None]
    query_blocks = to_blocks(query, block_count, head_count)
    decay_blocks = to_blocks(log_decay, block_count, head_count)
    key_blocks = to_blocks(opened, block_count, head_count)
    value_blocks = to_blocks(values, block_count, head_count)
    causal = jnp.tril(jnp.ones((SPAN, SPAN), jnp.bool_))
    inner_block_output = jnp.cumsum(decay_blocks, axis=2)
    block_decay_total = inner_block_output[:, :, -1, :]
    decayed_query = query_blocks * jnp.exp(inner_block_output)
    scores = jnp.einsum(
        "bhtk,bhsk->bhts",
        decayed_query,
        key_blocks * jnp.exp(-inner_block_output),
        precision=EXACT_MATMUL,
    )
    scores = jnp.where(causal, scores, 0.0)
    received_output = jnp.einsum("bhts,bhsv->bhtv", scores, value_blocks, precision=EXACT_MATMUL)
    growth_factor = jnp.einsum(
        "bhsk,bhsv->bhkv",
        key_blocks * jnp.exp(block_decay_total[:, :, None, :] - inner_block_output),
        value_blocks,
        precision=EXACT_MATMUL,
    )
    fading = jnp.exp(block_decay_total)

    def carry_step(state_matrix, item):
        return (item[0][:, :, None] * state_matrix + item[1], state_matrix)

    empty_state = jnp.zeros((head_count, RDIM, RDIM), jnp.float32)
    local_state, block_starts = lax.scan(carry_step, empty_state, (fading, growth_factor))
    received_output = received_output + jnp.einsum(
        "bhtk,bhkv->bhtv", decayed_query, block_starts, precision=EXACT_MATMUL
    )
    earlier_total = jnp.cumsum(block_decay_total, axis=0) - block_decay_total
    decay_from_start = query_blocks * jnp.exp(inner_block_output + earlier_total[:, :, None, :])
    device_fade = jnp.exp(jnp.sum(block_decay_total, axis=0))
    reach = 2**GROUPS - 1
    rim = pooled_in[row_count - reach :]
    unit_fade = jnp.ones((head_count, RDIM), jnp.float32)
    previous = passed_along(rim, "sp", 1)
    carried_fade, carried_state = prefix(
        (device_fade, local_state), "sp", chain, (unit_fade, empty_state)
    )
    received_output = received_output + jnp.einsum(
        "fuoy,uyi->fuoi", decay_from_start, carried_state, precision=EXACT_MATMUL
    )
    received_output = received_output.transpose(0, 2, 1, 3).reshape(row_count, head_count, RDIM)
    spread = lax.rsqrt(
        jnp.mean(received_output * received_output, axis=-1, keepdims=True) + EPSILON
    )
    recur_mixed = (
        (received_output * spread * out_gain).astype(jnp.bfloat16).reshape(row_count, recur_cols)
    )
    group = lax.axis_index("tp")
    padded = jnp.concatenate([previous, pooled_in], axis=0).astype(jnp.float32)
    results = window_sums(padded, GROUPS, reach)
    window_sum = results[GROUPS - 1]
    for level in range(GROUPS - 1):
        window_sum = jnp.where(group == level, results[level], window_sum)
    width = jnp.left_shift(jnp.int32(2), group)
    position = lax.axis_index("sp") * row_count + jnp.arange(row_count, dtype=jnp.int32)
    divisor = jnp.minimum(position + 1, width).astype(jnp.float32)[:, None]
    pool_mixed = (window_sum / divisor - pooled_in.astype(jnp.float32)).astype(jnp.bfloat16)
    out_pool, out_recur = (
        lax.all_gather(pool_out_weight, "sp", axis=1, tiled=True),
        lax.all_gather(recur_out_weight, "sp", axis=1, tiled=True),
    )
    partial_value = jnp.dot(pool_mixed, out_pool, preferred_element_type=jnp.float32)
    return lax.psum_scatter(
        (
            partial_value + jnp.dot(recur_mixed, out_recur, preferred_element_type=jnp.float32)
        ).astype(jnp.bfloat16),
        "tp",
        scatter_dimension=0,
        tiled=True,
    )


def solution(mesh):
    in_specs = (
        P(("sp", "tp"), None),
        P(),
        P("sp", "tp"),
        P("sp", "tp"),
        P("sp", "tp"),
        P("sp", "tp"),
        P("tp"),
        P("tp", "sp"),
        P(),
        P("tp", "sp"),
        P("tp", "sp"),
    )
    out_specs = P(("sp", "tp"), None)
    return jax.shard_map(local, mesh=mesh, in_specs=in_specs, out_specs=out_specs, check_vma=False)
```

profile of v0, /device:TPU:0, one launch (start us, length us, event | category | flops | bytes accessed | tf_op | source)
XLA Modules:
  0.0 273.9 jit_solution(6150586459145285040)
XLA Ops:
  6.5 1.3 fusion.7
  7.8 2.0 fusion.9
  9.9 2.0 pad_maximum_fusion
  11.9 0.7 all-gather.13.cloned.1.call-update
  12.9 22.4 %all-gather.9.cloned.1.call-done = bf16[512,2048]{1,0:T(8,128)(2,1)} async-done(((bf16[128,2048]{1,0:T(8,128)(2,1)}), bf16[512,2048]{1,0:T(8,128)(2,1)}) %all-gather.9.cloned.1.call-update) | async-done | bytes 2097168 | tf_op jit(solution)/shard_map/all_gather | solution.py:75
  35.3 74.9 %all-gather.11.cloned.1.call-done = bf16[2048,1024]{1,0:T(8,128)(2,1)} async-done(((bf16[256,1024]{1,0:T(8,128)(2,1)}), bf16[2048,1024]{1,0:T(8,128)(2,1)}) %all-gather.11.cloned.1.call-update) | async-done | bytes 4194320 | tf_op jit(solution)/shard_map/all_gather | solution.py:68
  110.2 4.3 %fusion.2 = bf16[512,768]{1,0:T(8,128)(2,1)S(1)} fusion(bf16[512,2048]{1,0:T(8,128)(2,1)} %all-gather.9.cloned.1.call-done, bf16[2048,1024]{1,0:T(8,128)(2,1)} %all-gather.11.cloned.1.call-done), kind=kOutput, calls=%fused_computation.8 | convolution fusion | flops 1611005952 | bytes 6029312 | tf_op jit(solution)/shard_map/dot_general | solution.py:79
  116.2 1.5 bitcast_multiply_fusion.4
  117.7 1.0 fusion.21
  118.7 6.6 %while.26 = (s32[]{:T(128)}, f32[2,128,128]{2,1,0:T(8,128)S(1)}, f32[8,2,128,128]{3,2,1,0:T(8,128)}, f32[8,2,128]{2,0,1:T(8,128)S(1)}, f32[8,2,128,128]{3,2,1,0:T(8,128)S(1)}, /*index=5*/s32[]{:T(128)}, s32[]{:T(128)}) while((s32[]{:T(128)}, f32[2,128,128]{2,1,0:T(8,128)S(1)}, f32[8,2,128,128]{3,2,1,0:T(8,128)}, ...), condition=%wide.region_3.4_spmd.clone, body=%wide.region_2.3_spmd.clone.sunk | while | flops 131075 | bytes 658540 | solution.py:121
  118.7 0.7 bitcast_dynamic-update-slice_fusion.2
  120.4 0.7 bitcast_dynamic-update-slice_fusion.2
  122.9 0.7 bitcast_dynamic-update-slice_fusion.2
  126.7 2.6 convolution_convert_fusion
  129.3 2.5 collective-permute-start
  131.8 1.2 convolution_select_fusion
  133.4 18.6 %all-gather.2 = f32[8,2,128]{2,1,0:T(2,128)S(1)} all-gather(f32[1,2,128]{2,1,0:T(2,128)S(1)} %exponential_bitcast_fusion), channel_id=2, replica_groups=mesh['sp'=8,'tp'=4] {'sp'}, dimensions={0}, use_global_device_ids=true | all-gather | bytes 9216 | tf_op jit(solution)/shard_map/all_gather | solution.py:21
  152.3 4.1 %fusion.30 = f32[512,2048]{1,0:T(8,128)} fusion(bf16[256,2048]{1,0:T(8,128)(2,1)} %all-gather.13.cloned.1.call-done, bf16[512,256]{1,0:T(8,128)(2,1)S(1)} %convolution_convert_fusion, f32[520,256]{1,0:T(8,128)S(1)} %slice_add_fusion.2, f32[526,256]{1,0:T(8,128)S(1)} %slice_add_fusion.1, f32[524,256]{1,0:T(8,128)S(1)} %slice_add_fusion, ...), kind=kOutput, calls=%fused_computation.54 | convolution fusion | flops 537919488 | bytes 7604227 | tf_op jit(solution)/shard_map/dot_general | solution.py:159
  156.3 35.2 %all-gather.17.cloned.1.call-done = f32[16,128,128]{2,1,0:T(8,128)} async-done(((f32[2,128,128]{2,1,0:T(8,128)}), f32[16,128,128]{2,1,0:T(8,128)}) %all-gather.17.cloned.1.call-update) | async-done | bytes 1048592 | tf_op jit(solution)/shard_map/all_gather | solution.py:21
  191.7 0.7 convolution_bitcast_fusion
  192.4 2.6 multiply_reduce_fusion
  195.6 36.0 %all-gather.15.cloned.1.call-done = bf16[256,2048]{1,0:T(8,128)(2,1)} async-done(((bf16[256,256]{1,0:T(8,128)(2,1)}), bf16[256,2048]{1,0:T(8,128)(2,1)}) %all-gather.15.cloned.1.call-update) | async-done | bytes 1048592 | tf_op jit(solution)/shard_map/all_gather | solution.py:157
  232.1 4.6 %add_convert_fusion = bf16[512,2048]{1,0:T(8,128)(2,1)} fusion(f32[512,2048]{1,0:T(8,128)} %fusion.30, bf16[256,2048]{1,0:T(8,128)(2,1)} %all-gather.15.cloned.1.call-done, f32[64,8,2,128]{3,2,1,0:T(2,128)S(1)} %bitcast.79, f32[64,8,2,128]{3,2,1,0:T(2,128)S(1)} %bitcast.78, f32[256]{0:T(256)S(1)} %broadcast_bitcast_fusion), kind=kOutput, calls=%fused_computation.5 | convolution fusion | flops 539361280 | bytes 8389632 | tf_op jit(solution)/shard_map/dot_general | solution.py:162
  236.7 30.3 %reduce-scatter.2.cloned.1.call-done = bf16[128,2048]{1,0:T(8,128)(2,1)} async-done(((bf16[512,2048]{1,0:T(8,128)(2,1)}), bf16[128,2048]{1,0:T(8,128)(2,1)}) %reduce-scatter.2.cloned.1.call-update) | async-done | bytes 524304 | tf_op jit(solution)/shard_map/reduce_scatter | solution.py:160
  (75 shorter events, 9.5 us)
Async XLA Ops:
  6.5 120.1 %copy-start = (f32[128]{0:T(128)S(1)}, f32[128]{0:T(128)}, u32[]{:S(2)}) copy-start(f32[128]{0:T(128)} %param.23) | copy-start | bytes 1540
  6.5 6.2 %copy-start.3 = (f32[2,512]{1,0:T(2,128)S(1)}, f32[2,512]{1,0:T(2,128)}, u32[]{:S(2)}) copy-start(f32[2,512]{1,0:T(2,128)} %param.22) | copy-start | bytes 12292
  6.5 28.8 %all-gather.9.cloned.1.call-start = ((), (), s32[]{:S(2)}) async-start(), calls=%async_computation.1 | async-start | bytes 2621440 | tf_op jit(solution)/shard_map/all_gather | solution.py:75
  9.9 100.4 %all-gather.11.cloned.1.call-start = ((), (), s32[]{:S(2)}) async-start(), calls=%async_computation.2 | async-start | bytes 4718592 | tf_op jit(solution)/shard_map/all_gather | solution.py:68
  11.9 140.4 %all-gather.13.cloned.1.call-start = ((), (), s32[]{:S(2)}) async-start(), calls=%async_computation.3 | async-start | bytes 1179648 | tf_op jit(solution)/shard_map/all_gather | solution.py:156
  12.6 178.9 %all-gather.17.cloned.1.call-start = ((), (), s32[]{:S(2)}) async-start(), calls=%async_computation.6 | async-start | bytes 1179648 | tf_op jit(solution)/shard_map/all_gather | solution.py:21
  114.6 0.7 copy-start.4
  125.3 0.7 copy-start.1
  126.0 105.5 %all-gather.15.cloned.1.call-start = ((), (), s32[]{:S(2)}) async-start(), calls=%async_computation.4 | async-start | bytes 1179648 | tf_op jit(solution)/shard_map/all_gather | solution.py:157
  126.6 140.5 %reduce-scatter.2.cloned.1.call-start = ((), (), s32[]{:S(2)}) async-start(), calls=%async_computation.5 | async-start | bytes 2621440 | tf_op jit(solution)/shard_map/reduce_scatter | solution.py:160
  129.3 22.7 %collective-permute-start = (bf16[15,256]{1,0:T(8,128)(2,1)S(1)}, bf16[15,256]{1,0:T(8,128)(2,1)S(1)}, u32[]{:S(2)}, u32[]{:S(2)}) collective-permute-start(bf16[15,256]{1,0:T(8,128)(2,1)S(1)} %slice.70), channel_id=1, source_target_pairs={{0,4},{4,8},{8,12},{12,16},{16,20},{20,24},{24,28},{1,5},{5,9},{9,... | collective-permute-start | bytes 23048 | tf_op jit(solution)/shard_map/ppermute | solution.py:16
  152.2 39.5 %copy-start.2 = (f32[8,2,64,128]{3,0,1,2:T(8,128)S(1)}, f32[8,2,64,128]{3,0,1,2:T(8,128)}, u32[]{:S(2)}) copy-start(f32[8,2,64,128]{3,0,1,2:T(8,128)} %get-tuple-element.146) | copy-start | bytes 1572868
Sparse Core Ops, SparseCore 0:
  10.0 25.2 all-gather.8
  37.4 72.7 all-gather.10
  112.3 37.9 all-gather.12
  152.2 39.1 all-gather.16
  193.4 38.0 all-gather.14
  236.8 30.1 reduce-scatter.1
where the time goes:
time: 274 us
  waiting for transfers between devices  200 us (73%)
  matrix products  21.4 us (8%)
  blocking collectives  18.6 us (7%)
  other arithmetic  14 us (5%)
  between operations  13.8 us (5%)
  local copies, waits for them, and re-layouts  2.88 us (1%)
    all_gather x1, waiting for transfers between devices, local(): whole_in = lax.all_gather(local_in, 'sp', axis=0, tiled=True)  74.9 us
    all_gather x1, waiting for transfers between devices, local(): lax.all_gather(recur_out_weight, 'sp', axis=1, tiled=True)  36 us
    all_gather x1, waiting for transfers between devices, prefix(): gathered = jax.tree.map(lambda a: lax.all_gather(a, axis), part)  35.2 us
    reduce_scatter x1, waiting for transfers between devices, local(): lax.psum_scatter((partial_value + jnp.dot(recur_mixed, out_recur, preferr...  30.3 us
    all_gather x1, waiting for transfers between devices, local(): lax.all_gather(normed, 'tp', axis=0, tiled=True)  22.4 us
    all_gather x1, blocking collectives, prefix(): gathered = jax.tree.map(lambda a: lax.all_gather(a, axis), part)  18.6 us
  transfers between devices with their start and end apart: 7, of which 5 were waited for; matrix products, arithmetic and copies ran while one was open for 11% of the time, Pallas kernels for 0%

commit v1 on v0

--- a/solution.py
+++ b/solution.py
@@ -154,7 +154,9 @@
     pool_mixed = (window_sum / divisor - pooled_in.astype(jnp.float32)).astype(jnp.bfloat16)
     out_pool, out_recur = (
         lax.all_gather(pool_out_weight, "sp", axis=1, tiled=True),
-        lax.all_gather(recur_out_weight, "sp", axis=1, tiled=True),
+        jnp.concatenate(
+            lax.all_to_all(jnp.stack([recur_out_weight] * lax.axis_size("sp")), "sp", 0, 0), axis=1
+        ),
     )
     partial_value = jnp.dot(pool_mixed, out_pool, preferred_element_type=jnp.float32)
     return lax.psum_scatter(

time: 274 us -> 245 us (0.89)
  waiting for transfers between devices: 200 us -> 150 us
  local copies, waits for them, and re-layouts: 2.88 us -> 11.4 us
  starting transfers between devices: 2.66 us -> 10.4 us
  other arithmetic: 14 us -> 18.5 us
    all_gather x1 -> x0, waiting for transfers between devices: 36 us -> none  [local(): lax.all_gather(recur_out_weight, 'sp', axis=1, tiled=True)]
    all_gather x1, waiting for transfers between devices: 35.2 us -> 24.1 us  [prefix(): gathered = jax.tree.map(lambda a: lax.all_gather(a, axis), part)]
    all_gather x1, waiting for transfers between devices: 22.4 us -> 12.7 us  [local(): lax.all_gather(normed, 'tp', axis=0, tiled=True)]
    all_to_all x0 -> x1, starting transfers between devices: none -> 7.28 us  [local(): lax.all_to_all(jnp.stack([recur_out_weight] * lax.axis_size('sp')), 'sp',...]
    reduce_scatter x1, waiting for transfers between devices: 30.3 us -> 37.5 us  [local(): lax.psum_scatter((partial_value + jnp.dot(recur_mixed, out_recur, preferr...]
    dynamic_slice x8, local copies, waits for them, and re-layouts: 0.06 us -> 5.65 us  [local(): lax.scan(carry_step, empty_state, (fading, growth_factor))]
  transfers between devices with their start and end apart: 7 -> 7, of which waited for: 5 -> 4; matrix products, arithmetic and copies ran while one was open for 11% -> 18% of each run, Pallas kernels for 0% -> 0%
where the time goes in v1:
time: 245 us; the launch traced here: 244 us
  waiting for transfers between devices  150 us (61%)
  matrix products  21.6 us (9%)
  other arithmetic  18.5 us (8%)
  blocking collectives  17.8 us (7%)
  between operations  13.5 us (6%)
  local copies, waits for them, and re-layouts  11.4 us (5%)
  starting transfers between devices  10.4 us (4%)
    all_gather x1, waiting for transfers between devices, local(): whole_in = lax.all_gather(local_in, 'sp', axis=0, tiled=True)  74.9 us
    reduce_scatter x1, waiting for transfers between devices, local(): lax.psum_scatter((partial_value + jnp.dot(recur_mixed, out_recur, preferr...  37.5 us
    all_gather x1, waiting for transfers between devices, prefix(): gathered = jax.tree.map(lambda a: lax.all_gather(a, axis), part)  24.1 us
    all_gather x1, blocking collectives, prefix(): gathered = jax.tree.map(lambda a: lax.all_gather(a, axis), part)  17.8 us
    all_gather x1, waiting for transfers between devices, local(): lax.all_gather(normed, 'tp', axis=0, tiled=True)  12.7 us
    all_to_all x1, starting transfers between devices, local(): lax.all_to_all(jnp.stack([recur_out_weight] * lax.axis_size('sp')), 'sp',...  7.28 us
    dynamic_slice x8, local copies, waits for them, and re-layouts, local(): lax.scan(carry_step, empty_state, (fading, growth_factor))  5.65 us
    dynamic_update_slice x8, other arithmetic, local(): lax.scan(carry_step, empty_state, (fading, growth_factor))  5.28 us
  transfers between devices with their start and end apart: 7, of which 4 were waited for; matrix products, arithmetic and copies ran while one was open for 18% of the time, Pallas kernels for 0%

profile of v1, /device:TPU:0, one launch (start us, length us, event | category | flops | bytes accessed | tf_op | source)
XLA Modules:
  0.0 243.7 jit_solution(14772320486867762685)
XLA Ops:
  6.5 1.3 fusion.7
  7.8 2.0 fusion.9
  9.9 2.0 pad_maximum_fusion
  12.0 1.1 stack.2
  13.1 7.3 %all-to-all-start = ((bf16[8,256,256]{1,2,0:T(8,128)(2,1)}), bf16[8,256,256]{1,2,0:T(8,128)(2,1)S(1)}, u32[]{:S(2)}, u32[]{:S(2)}) async-start(bf16[8,256,256]{1,2,0:T(8,128)(2,1)} %stack.2), calls=%async_computation | async-start | bytes 2097152 | tf_op jit(solution)/shard_map/all_to_all | solution.py:158
  22.6 12.7 %all-gather.8.cloned.1.call-done = bf16[512,2048]{1,0:T(8,128)(2,1)} async-done(((bf16[128,2048]{1,0:T(8,128)(2,1)}), bf16[512,2048]{1,0:T(8,128)(2,1)}) %all-gather.8.cloned.1.call-update) | async-done | bytes 2097168 | tf_op jit(solution)/shard_map/all_gather | solution.py:75
  35.3 74.9 %all-gather.10.cloned.1.call-done = bf16[2048,1024]{1,0:T(8,128)(2,1)} async-done(((bf16[256,1024]{1,0:T(8,128)(2,1)}), bf16[2048,1024]{1,0:T(8,128)(2,1)}) %all-gather.10.cloned.1.call-update) | async-done | bytes 4194320 | tf_op jit(solution)/shard_map/all_gather | solution.py:68
  110.3 4.3 %fusion.2 = bf16[512,768]{1,0:T(8,128)(2,1)S(1)} fusion(bf16[512,2048]{1,0:T(8,128)(2,1)} %all-gather.8.cloned.1.call-done, bf16[2048,1024]{1,0:T(8,128)(2,1)} %all-gather.10.cloned.1.call-done), kind=kOutput, calls=%fused_computation.8 | convolution fusion | flops 1611005952 | bytes 6029312 | tf_op jit(solution)/shard_map/dot_general | solution.py:79
  115.2 1.3 fusion.16
  117.2 2.6 %convolution_convert_fusion = bf16[512,256]{1,0:T(8,128)(2,1)S(1)} fusion(bf16[512,2048]{1,0:T(8,128)(2,1)} %all-gather.8.cloned.1.call-done, bf16[2048,1024]{1,0:T(8,128)(2,1)} %all-gather.10.cloned.1.call-done), kind=kOutput, calls=%fused_computation.16 | convolution fusion | flops 537001984 | bytes 3407872 | tf_op jit(solution)/shard_map/dot_general | solution.py:74
  120.5 3.0 %collective-permute-start = (bf16[15,256]{1,0:T(8,128)(2,1)}, bf16[15,256]{1,0:T(8,128)(2,1)}, u32[]{:S(2)}, u32[]{:S(2)}) collective-permute-start(bf16[15,256]{1,0:T(8,128)(2,1)} %slice.70), channel_id=1, source_target_pairs={{0,4},{4,8},{8,12},{12,16},{16,20},{20,24},{24,28},{1,5},{5,9},{9,... | collective-permute-start | bytes 23048 | tf_op jit(solution)/shard_map/ppermute | solution.py:16
  123.6 1.2 slice_bitcast_fusion
  124.7 1.1 reshape.90
  125.8 2.6 %bitcast_multiply_fusion.3 = (f32[8,2,64,128]{3,0,1,2:T(8,128)S(1)}, f32[8,2,64,128]{3,0,1,2:T(8,128)}, f32[8,2,64,128]{3,0,1,2:T(8,128)S(1)}, f32[8,2,64,128]{3,0,1,2:T(8,128)S(1)}) fusion(f32[8,2,64,128]{3,0,1,2:T(8,128)S(1)} %fusion.16, f32[8,64,2,128]{3,2,1,0:T(2,128)} %reshape.90, f32[8,2,128]{2,0,1:T(8,128)} %get-tuple-element.143, ...), kind=kLoop, calls=%fused_computation.36 | loop fusion | flops 1048576 | bytes 3687424 | tf_op jit(solution)/shard_map/mul | solution.py:100
  129.4 12.1 %while.26 = (s32[]{:T(128)}, f32[2,128,128]{2,1,0:T(8,128)S(1)}, f32[8,2,128,128]{3,2,1,0:T(8,128)}, f32[8,2,128]{2,0,1:T(8,128)}, f32[8,2,128,128]{3,2,1,0:T(8,128)S(1)}, /*index=5*/s32[]{:T(128)}, s32[]{:T(128)}) while((s32[]{:T(128)}, f32[2,128,128]{2,1,0:T(8,128)S(1)}, f32[8,2,128,128]{3,2,1,0:T(8,128)}, ...), condition=%wide.region_3.4_spmd.clone, body=%wide.region_2.3_spmd.clone.sunk | while | flops 131075 | bytes 658540 | solution.py:121
  142.3 1.2 convolution_select_fusion
  143.5 1.2 fusion.33
  144.7 17.8 %all-gather.2 = f32[8,2,128]{2,1,0:T(2,128)S(1)} all-gather(f32[1,2,128]{2,1,0:T(2,128)S(1)} %exponential_bitcast_fusion), channel_id=2, replica_groups=mesh['sp'=8,'tp'=4] {'sp'}, dimensions={0}, use_global_device_ids=true | all-gather | bytes 9216 | tf_op jit(solution)/shard_map/all_gather | solution.py:21
  163.5 4.0 %fusion.28 = f32[512,2048]{1,0:T(8,128)} fusion(bf16[256,2048]{1,0:T(8,128)(2,1)} %all-gather.12.cloned.1.call-done, bf16[512,256]{1,0:T(8,128)(2,1)S(1)} %copy-done.3, f32[520,256]{1,0:T(8,128)S(1)} %slice_add_fusion.2, f32[526,256]{1,0:T(8,128)S(1)} %slice_add_fusion.1, f32[524,256]{1,0:T(8,128)S(1)} %slice_add_fusion, f32[512]{0:T(512)S(1)} %copy-done.6, ...), kind=kOutput, calls=%fused_computation.52 | convolution fusion | flops 537919488 | bytes 7604227 | tf_op jit(solution)/shard_map/dot_general | solution.py:161
  167.5 24.1 %all-gather.14.cloned.1.call-done = f32[16,128,128]{2,1,0:T(8,128)} async-done(((f32[2,128,128]{2,1,0:T(8,128)}), f32[16,128,128]{2,1,0:T(8,128)}) %all-gather.14.cloned.1.call-update) | async-done | bytes 1048592 | tf_op jit(solution)/shard_map/all_gather | solution.py:21
  191.8 1.7 convolution_bitcast_fusion
  193.6 1.3 multiply_reduce_fusion
  195.3 4.3 %add_convert_fusion = bf16[512,2048]{1,0:T(8,128)(2,1)} fusion(f32[512,2048]{1,0:T(8,128)} %fusion.28, bf16[256,2048]{0,1:T(8,128)(2,1)S(1)} %bitcast.70, bf16[64,8,2,128]{3,2,1,0:T(2,128)(2,1)S(1)} %bitcast.71), kind=kOutput, calls=%fused_computation.5 | convolution fusion | flops 538968064 | bytes 7602176 | tf_op jit(solution)/shard_map/dot_general | solution.py:164
  199.7 37.5 %reduce-scatter.2.cloned.1.call-done = bf16[128,2048]{1,0:T(8,128)(2,1)} async-done(((bf16[512,2048]{1,0:T(8,128)(2,1)}), bf16[128,2048]{1,0:T(8,128)(2,1)}) %reduce-scatter.2.cloned.1.call-update) | async-done | bytes 524304 | tf_op jit(solution)/shard_map/reduce_scatter | solution.py:162
  (86 shorter events, 19.6 us)
Async XLA Ops:
  6.5 5.4 %copy-start.5 = (bf16[256,256]{1,0:T(8,128)(2,1)S(1)}, bf16[256,256]{1,0:T(8,128)(2,1)}, u32[]{:S(2)}) copy-start(bf16[256,256]{1,0:T(8,128)(2,1)} %param.25) | copy-start | bytes 393220
  6.5 28.8 %all-gather.8.cloned.1.call-start = ((), (), s32[]{:S(2)}) async-start(), calls=%async_computation.2 | async-start | bytes 2621440 | tf_op jit(solution)/shard_map/all_gather | solution.py:75
  9.8 11.4 %copy-start.7 = (f32[2,512]{1,0:T(2,128)S(1)}, f32[2,512]{1,0:T(2,128)}, u32[]{:S(2)}) copy-start(f32[2,512]{1,0:T(2,128)} %param.22) | copy-start | bytes 12292
  9.9 100.4 %all-gather.10.cloned.1.call-start = ((), (), s32[]{:S(2)}) async-start(), calls=%async_computation.3 | async-start | bytes 4718592 | tf_op jit(solution)/shard_map/all_gather | solution.py:68
  13.1 182.2 %all-to-all-start = ((bf16[8,256,256]{1,2,0:T(8,128)(2,1)}), bf16[8,256,256]{1,2,0:T(8,128)(2,1)S(1)}, u32[]{:S(2)}, u32[]{:S(2)}) async-start(bf16[8,256,256]{1,2,0:T(8,128)(2,1)} %stack.2), calls=%async_computation | async-start | bytes 2097152 | tf_op jit(solution)/shard_map/all_to_all | solution.py:158
  20.4 143.1 %all-gather.12.cloned.1.call-start = ((), (), s32[]{:S(2)}) async-start(), calls=%async_computation.4 | async-start | bytes 1179648 | tf_op jit(solution)/shard_map/all_gather | solution.py:156
  21.1 170.5 %all-gather.14.cloned.1.call-start = ((), (), s32[]{:S(2)}) async-start(), calls=%async_computation.6 | async-start | bytes 1179648 | tf_op jit(solution)/shard_map/all_gather | solution.py:21
  114.6 0.7 copy-start.9
  119.8 3.6 %copy-start.2 = (bf16[512,256]{1,0:T(8,128)(2,1)}, bf16[512,256]{1,0:T(8,128)(2,1)S(1)}, u32[]{:S(2)}) copy-start(bf16[512,256]{1,0:T(8,128)(2,1)S(1)} %convolution_convert_fusion) | copy-start | bytes 786436
  120.5 42.0 %collective-permute-start = (bf16[15,256]{1,0:T(8,128)(2,1)}, bf16[15,256]{1,0:T(8,128)(2,1)}, u32[]{:S(2)}, u32[]{:S(2)}) collective-permute-start(bf16[15,256]{1,0:T(8,128)(2,1)} %slice.70), channel_id=1, source_target_pairs={{0,4},{4,8},{8,12},{12,16},{16,20},{20,24},{24,28},{1,5},{5,9},{9,... | collective-permute-start | bytes 23048 | tf_op jit(solution)/shard_map/ppermute | solution.py:16
  129.4 15.2 %copy-start.8 = (f32[2,128]{1,0:T(2,128)S(1)}, f32[2,128]{1,0:T(2,128)}, u32[]{:S(2)}) copy-start(f32[2,128]{1,0:T(2,128)} %get-tuple-element.142) | copy-start | bytes 3076
  141.5 0.7 copy-start
  141.5 21.0 %copy-start.3 = (bf16[512,256]{1,0:T(8,128)(2,1)S(1)}, bf16[512,256]{1,0:T(8,128)(2,1)}, u32[]{:S(2)}) copy-start(bf16[512,256]{1,0:T(8,128)(2,1)} %copy-done.2) | copy-start | bytes 786436
  142.2 95.0 %reduce-scatter.2.cloned.1.call-start = ((), (), s32[]{:S(2)}) async-start(), calls=%async_computation.5 | async-start | bytes 2621440 | tf_op jit(solution)/shard_map/reduce_scatter | solution.py:162
  144.6 18.8 %copy-start.6 = (f32[512]{0:T(512)S(1)}, f32[512]{0:T(512)}, u32[]{:S(2)}) copy-start(f32[512]{0:T(512)} %minimum_convert_fusion) | copy-start | bytes 6148
  167.5 26.0 %copy-start.1 = (f32[8,2,64,128]{3,2,1,0:T(8,128)S(1)}, f32[8,2,64,128]{3,2,1,0:T(8,128)}, u32[]{:S(2)}) copy-start(f32[8,2,64,128]{3,2,1,0:T(8,128)} %fusion.33) | copy-start | bytes 1572868
  167.5 26.0 %copy-start.4 = (f32[8,2,128,128]{3,2,1,0:T(8,128)S(1)}, f32[8,2,128,128]{3,2,1,0:T(8,128)}, u32[]{:S(2)}) copy-start(f32[8,2,128,128]{3,2,1,0:T(8,128)} %get-tuple-element.77) | copy-start | bytes 3145732
  191.6 3.2 %copy-start.10 = (f32[128]{0:T(128)S(1)}, f32[128]{0:T(128)}, u32[]{:S(2)}) copy-start(f32[128]{0:T(128)} %param.23) | copy-start | bytes 1540
Sparse Core Ops, SparseCore 0:
  10.0 25.2 all-gather.7
  37.4 72.7 all-gather.9
  112.3 37.9 all-gather.11
  152.3 39.2 all-gather.13
  199.8 37.3 reduce-scatter.1
